TPU v7x, 32 devices: a whole 2x2x4 slice. The times are simulated.
32 devices in a mesh: ep: 8 (over z, x), tp: 4 (over y, core).
Axes of the slice: x: 2, y: 2, z: 4, core: 2. Of those that a mesh axis runs over, the one named last changes fastest.
Arguments:
- resid: bfloat16 [256, 2048], P('ep'), may hold values from -6 to 6
- norm_gain: bfloat16 [2048], replicated, may hold values from 0.099609375 to 1.8984375
- w_query: bfloat16 [2048, 1024], P(None, 'tp'), may hold values from -0.125 to 0.125
- w_key: bfloat16 [2048, 1024], P(None, 'tp'), may hold values from -0.125 to 0.125
- w_value: bfloat16 [2048, 1024], P(None, 'tp'), may hold values from -0.125 to 0.125
- w_gate: bfloat16 [2048, 1024], P(None, 'tp'), may hold values from -0.125 to 0.125
- head_gain: bfloat16 [1024], P('tp'), may hold values from 0.099609375 to 1.8984375
- w_output: bfloat16 [1024, 2048], P('tp'), may hold values from -0.1875 to 0.1875
- state: float32 [256, 8, 128, 128], P('ep', 'tp'), may hold values from -0.6 to 0.6
- positions: int32 [256], P('ep'), may hold values from 1024 to 8191
- ffn_gain: bfloat16 [2048], replicated, may hold values from 0.099609375 to 1.8984375
- w_mix: bfloat16 [2048], replicated, may hold values from -0.125 to 0.125
- dense_gate: bfloat16 [2048, 5632], P('tp', 'ep'), may hold values from -0.125 to 0.125
- dense_up: bfloat16 [2048, 5632], P('tp', 'ep'), may hold values from -0.125 to 0.125
- dense_down: bfloat16 [5632, 2048], P('ep', 'tp'), may hold values from -0.109375 to 0.109375
- routes: int32 [256, 2], P('ep'), may hold values from 0 to 7, all different within a row; in each aligned block of 32 rows (0 to 31, 32 to 63, ...) at most 16 rows name the same one
- route_weight: bfloat16 [256, 2], P('ep'), may hold values from 0.19921875 to 1
- expert_gate: bfloat16 [8, 2048, 4096], P('ep', None, 'tp'), may hold values from -0.125 to 0.125
- expert_up: bfloat16 [8, 2048, 4096], P('ep', None, 'tp'), may hold values from -0.125 to 0.125
- expert_down: bfloat16 [8, 4096, 2048], P('ep', 'tp'), may hold values from -0.09375 to 0.09375
Outputs:
- final: bfloat16 [256, 2048], P('ep', 'tp')
- new_state: float32 [256, 8, 128, 128], P('ep', 'tp')
Inputs may be any that keep to these rules, and one draw needn't show every extreme that they name: `routes`: each row names 2 different experts; in the rows of one index of ep no expert is named by more than 16 rows, a bound that some block reaches; every expert is named by some row.
All inputs are finite; a program needn't handle non-finite values.
Results may differ from a plain program's by a relative error of at most 0.018.
Values may be sent and summed in bfloat16 or wider, within the bound.
A program may use at most 64 MiB of HBM per device.

v0:
```python
import jax
import jax.numpy as jnp
from jax import lax
from jax.sharding import PartitionSpec as P

EPSILON = 1e-06
THETA = 10000.0


def rms_norm(inputs, scaling):
    square = jnp.mean(inputs * inputs, axis=-1, keepdims=True)
    return inputs * lax.rsqrt(square + EPSILON) * scaling.astype(jnp.float32)


def rotate(inputs, places):
    halfway = inputs.shape[-1] // 2
    inverse = THETA ** (-jnp.arange(halfway, dtype=jnp.float32) / halfway)
    angles = places.astype(jnp.float32)[:, None] * inverse[None, :]
    cosine = jnp.cos(angles)[:, None, :]
    sine_of = jnp.sin(angles)[:, None, :]
    former = inputs[..., :halfway]
    latter = inputs[..., halfway:]
    return jnp.concatenate(
        [former * cosine - latter * sine_of, former * sine_of + latter * cosine], axis=-1
    )


def retain(queries, keys_in, values_in, gating, memory, places, head_first, head_gain):
    seqs_here = queries.shape[0]
    heads_here = memory.shape[1]
    head_size = memory.shape[2]
    head_shape = (seqs_here, heads_here, head_size)
    query_rot = rotate(queries.astype(jnp.float32).reshape(head_shape), places)
    key_rot = rotate(keys_in.astype(jnp.float32).reshape(head_shape), places) * head_size ** (-0.5)
    value_heads = values_in.astype(jnp.float32).reshape(head_shape)
    head_index = head_first + jnp.arange(heads_here, dtype=jnp.float32)
    decays = 1.0 - jnp.exp2(-1.0 - 1.5 * head_index)
    within = jnp.sum(query_rot * key_rot, axis=-1, keepdims=True) * value_heads
    carried = (
        jnp.einsum("shd,shde->she", query_rot, memory, precision=lax.Precision.HIGHEST)
        * decays[None, :, None]
    )
    mixture = within + carried
    new_memory = (
        decays[None, :, None, None] * memory + key_rot[:, :, :, None] * value_heads[:, :, None, :]
    )
    centre = jnp.mean(mixture, axis=-1, keepdims=True)
    spread = jnp.mean(jnp.square(mixture - centre), axis=-1, keepdims=True)
    normed = ((mixture - centre) * lax.rsqrt(spread + EPSILON)).reshape(
        seqs_here, heads_here * head_size
    )
    normed = normed * head_gain.astype(jnp.float32)
    output = (jax.nn.silu(gating.astype(jnp.float32)) * normed).astype(jnp.bfloat16)
    return (output, new_memory)


def expert_hidden(chosen, gate_weight, up_weight):
    gate_value = jnp.dot(chosen, gate_weight, preferred_element_type=jnp.float32)
    up_value = jnp.dot(chosen, up_weight, preferred_element_type=jnp.float32)
    return (jax.nn.silu(gate_value) * up_value).astype(jnp.bfloat16)


def padded_experts(
    normed_mid, routes, route_weight, expert_gate, expert_up, expert_down, capacity, experts_all
):
    seq_dev, model_width = normed_mid.shape
    top_count = routes.shape[1]
    flat_ids = routes.reshape(-1)
    expert_ids = jnp.arange(experts_all, dtype=jnp.int32)
    onehot = (flat_ids[:, None] == expert_ids[None, :]).astype(jnp.int32)
    ranks = jnp.sum((jnp.cumsum(onehot, axis=0) - 1) * onehot, axis=1)
    slot_ids = flat_ids * capacity + ranks
    slot_range = jnp.arange(experts_all * capacity, dtype=jnp.int32)
    dispatch = (slot_range[:, None] == slot_ids[None, :]).astype(jnp.bfloat16)
    repeated = jnp.repeat(normed_mid, top_count, axis=0)
    outgoing = jnp.dot(dispatch, repeated, preferred_element_type=jnp.float32).astype(jnp.bfloat16)
    outgoing = outgoing.reshape(experts_all, capacity, model_width)
    arrived = lax.all_to_all(outgoing, "ep", split_axis=0, concat_axis=0, tiled=True)
    sources = arrived.shape[0]
    items = arrived.shape[1]
    hidden_e = expert_hidden(
        arrived.reshape(sources * items, model_width), expert_gate[0], expert_up[0]
    )
    partial_value = jnp.dot(hidden_e, expert_down[0], preferred_element_type=jnp.float32)
    summed = lax.psum_scatter(
        partial_value.astype(jnp.bfloat16), "tp", scatter_dimension=1, tiled=True
    )
    returned = lax.all_to_all(
        summed.reshape(sources, items, summed.shape[1]),
        "ep",
        split_axis=0,
        concat_axis=0,
        tiled=True,
    )
    flat_back = returned.reshape(experts_all * capacity, returned.shape[2])
    weighted = flat_back[slot_ids].astype(jnp.float32) * route_weight.reshape(-1)[:, None].astype(
        jnp.float32
    )
    return jnp.sum(weighted.reshape(seq_dev, top_count, weighted.shape[1]), axis=1)


def per_device(
    resid,
    norm_gain,
    w_query,
    w_key,
    w_value,
    w_gate,
    head_gain,
    w_output,
    state,
    positions,
    ffn_gain,
    w_mix,
    dense_gate,
    dense_up,
    dense_down,
    routes,
    route_weight,
    expert_gate,
    expert_up,
    expert_down,
):
    seq_dev = resid.shape[0]
    model_width = resid.shape[1]
    tp_count = lax.axis_size("tp")
    ep_count = lax.axis_size("ep")
    model_tp = model_width // tp_count
    tp_index = lax.axis_index("tp")
    normed_in = rms_norm(resid.astype(jnp.float32), norm_gain).astype(jnp.bfloat16)

    def project(weight):
        return jnp.dot(normed_in, weight, preferred_element_type=jnp.float32).astype(jnp.bfloat16)

    heads_here = state.shape[1]
    head_first = (tp_index * heads_here).astype(jnp.float32)
    retained, new_state = retain(
        project(w_query),
        project(w_key),
        project(w_value),
        project(w_gate),
        state,
        positions,
        head_first,
        head_gain,
    )
    partial_value = jnp.dot(retained, w_output, preferred_element_type=jnp.float32)
    attention = lax.psum(partial_value.astype(jnp.bfloat16), "tp").astype(jnp.float32)
    middle = resid.astype(jnp.float32) + attention
    normed_mid = rms_norm(middle, ffn_gain).astype(jnp.bfloat16)
    mixing = jax.nn.sigmoid(jnp.dot(normed_mid, w_mix[:, None], preferred_element_type=jnp.float32))

    def own_columns(matrix):
        return lax.dynamic_slice_in_dim(matrix, tp_index * model_tp, model_tp, 1)

    top_count = routes.shape[1]
    capacity = max(2, 2 * seq_dev * top_count // ep_count)
    dense_rows = lax.all_gather(own_columns(normed_mid), "ep", axis=0, tiled=True)
    moe_out = padded_experts(
        normed_mid, routes, route_weight, expert_gate, expert_up, expert_down, capacity, ep_count
    )
    gate_part = jnp.dot(dense_rows, dense_gate, preferred_element_type=jnp.float32)
    up_part = jnp.dot(dense_rows, dense_up, preferred_element_type=jnp.float32)
    gate_sum, up_sum = (
        lax.psum(gate_part.astype(jnp.bfloat16), "tp").astype(jnp.float32),
        lax.psum(up_part.astype(jnp.bfloat16), "tp").astype(jnp.float32),
    )
    dense_hidden = (jax.nn.silu(gate_sum) * up_sum).astype(jnp.bfloat16)
    dense_out = lax.psum_scatter(
        jnp.dot(dense_hidden, dense_down, preferred_element_type=jnp.float32).astype(jnp.bfloat16),
        "ep",
        scatter_dimension=0,
        tiled=True,
    ).astype(jnp.float32)
    final = (own_columns(middle) + moe_out + mixing * dense_out).astype(jnp.bfloat16)
    return (final, new_state)


def solution(mesh):
    in_specs = (
        P("ep", None),
        P(),
        P(None, "tp"),
        P(None, "tp"),
        P(None, "tp"),
        P(None, "tp"),
        P("tp"),
        P("tp", None),
        P("ep", "tp", None, None),
        P("ep"),
        P(),
        P(),
        P("tp", "ep"),
        P("tp", "ep"),
        P("ep", "tp"),
        P("ep", None),
        P("ep", None),
        P("ep", None, "tp"),
        P("ep", None, "tp"),
        P("ep", "tp", None),
    )
    out_specs = (P("ep", "tp"), P("ep", "tp", None, None))
    return jax.shard_map(
        per_device, mesh=mesh, in_specs=in_specs, out_specs=out_specs, check_vma=False
    )
```

profile of v0, /device:TPU:0, one launch (start us, length us, event | category | flops | bytes accessed | tf_op | source)
XLA Modules:
  0.0 234.7 jit_solution(9448984096883275482)
XLA Ops:
  7.3 0.7 convert_element_type.111
  8.0 1.0 fusion.40
  9.0 0.7 convert_element_type.115
  9.7 0.7 convert_element_type.106
  10.4 1.6 fusion.20
  12.1 1.7 fusion.19
  13.8 1.6 fusion.18
  16.0 5.3 %fusion.61 = f32[32,2,1,128]{3,2,1,0:T(1,128)S(1)} fusion(f32[32,2,128,1]{2,3,1,0:T(1,128)S(1)} %bitcast.72, f32[32,2,128,128]{3,2,1,0:T(8,128)} %param.28), kind=kOutput, calls=%fused_computation.95 | convolution fusion | flops 12582912 | bytes 4259840 | tf_op jit(solution)/shard_map/shd,shde->she/dot_general | solution.py:40
  21.3 0.2 fusion.60
  21.5 0.2 multiply_reduce_fusion.2
  21.9 1.5 convolution_convert_fusion.1
  23.8 0.2 select_reduce_fusion
  24.0 34.1 %all-reduce.4.cloned.1.call-done = bf16[32,2048]{1,0:T(8,128)(2,1)} async-done(((bf16[32,2048]{1,0:T(8,128)(2,1)}), bf16[32,2048]{1,0:T(8,128)(2,1)}) %all-reduce.4.cloned.1.call-update) | async-done | bytes 131088 | tf_op jit(solution)/shard_map/psum | solution.py:148
  58.1 1.1 convert_add_fusion
  59.1 1.0 multiply_convert_fusion
  60.4 1.1 convolution_convert_fusion
  61.5 5.5 %all-to-all-start = ((bf16[8,16,2048]{2,1,0:T(8,128)(2,1)}), bf16[8,16,2048]{2,1,0:T(8,128)(2,1)S(1)}, u32[]{:S(2)}, u32[]{:S(2)}) async-start(bf16[8,16,2048]{2,1,0:T(8,128)(2,1)} %bitcast.4), calls=%async_computation | async-start | bytes 1048576 | tf_op jit(solution)/shard_map/all_to_all | solution.py:78
  67.0 36.6 %all_gather.3 = bf16[256,512]{1,0:T(8,128)(2,1)S(1)} all-gather(bf16[32,512]{1,0:T(8,128)(2,1)S(1)} %constant_dynamic-slice_fusion), channel_id=1, replica_groups=mesh['ep'=8,'tp'=4] {'ep'}, dimensions={0}, use_global_device_ids=true | all-gather | bytes 294912 | tf_op jit(solution)/shard_map/all_gather | solution.py:158
  103.7 1.1 convolution_convert_fusion.2
  104.8 1.1 convolution_convert_fusion.3
  106.0 2.9 %fusion.5 = f32[128,1024]{1,0:T(8,128)S(1)} fusion(bf16[128,2048]{1,0:T(8,128)(2,1)S(1)} %bitcast.69, bf16[1,2048,1024]{2,1,0:T(8,128)(2,1)} %param.37), kind=kOutput, calls=%fused_computation.6 | convolution fusion | flops 536870912 | bytes 5242880 | tf_op jit(solution)/shard_map/dot_general | solution.py:58
  109.0 5.6 %fusion.7 = bf16[128,2048]{1,0:T(8,128)(2,1)} fusion(bf16[1,1024,2048]{2,1,0:T(8,128)(2,1)} %param.39, bf16[128,2048]{1,0:T(8,128)(2,1)S(1)} %bitcast.70, bf16[1,2048,1024]{2,1,0:T(8,128)(2,1)} %param.38, f32[128,1024]{1,0:T(8,128)S(1)} %fusion.5), kind=kOutput, calls=%fused_computation.9 | convolution fusion | flops 1074790400 | bytes 9961472 | tf_op jit(solution)/shard_map/dot_general | solution.py:84
  114.9 4.3 %multiply_add_fusion = f32[32,2,128,128]{3,2,1,0:T(8,128)} fusion(f32[32,2,128,128]{3,2,1,0:T(8,128)} %param.28, f32[32,2,128]{2,1,0:T(2,128)S(1)} %copy-done.6, f32[32,2,128]{2,1,0:T(2,128)S(1)} %copy-done.8, f32[2]{0:T(128)S(1)} %exponential_subtract_fusion), kind=kLoop, calls=%fused_computation.8 | loop fusion | flops 3145728 | bytes 8454152 | tf_op jit(solution)/shard_map/add | solution.py:45
  119.2 18.0 %all-reduce.6.cloned.1.call-done = (bf16[256,704]{0,1:T(8,128)(2,1)}, bf16[256,704]{0,1:T(8,128)(2,1)}) async-done(((bf16[256,704]{0,1:T(8,128)(2,1)}, bf16[256,704]{0,1:T(8,128)(2,1)}), (bf16[256,704]{0,1:T(8,128)(2,1)}, bf16[256,704]{0,1:T(8,128)(2,1)})) %all-reduce.6.cloned.1.call-update) | async-done | bytes 720912 | tf_op jit(solution)/shard_map/psum | solution.py:166
  137.2 2.2 convolution_convert_fusion.4
  139.5 21.9 %reduce-scatter.3.cloned.1.call-done = bf16[128,512]{1,0:T(8,128)(2,1)} async-done(((bf16[128,2048]{1,0:T(8,128)(2,1)}), bf16[128,512]{1,0:T(8,128)(2,1)}) %reduce-scatter.3.cloned.1.call-update) | async-done | bytes 131088 | tf_op jit(solution)/shard_map/reduce_scatter | solution.py:85
  161.4 5.5 %all-to-all-start.1 = ((bf16[8,16,512]{2,1,0:T(8,128)(2,1)}), bf16[8,16,512]{2,1,0:T(8,128)(2,1)S(1)}, u32[]{:S(2)}, u32[]{:S(2)}) async-start(bf16[8,16,512]{2,1,0:T(8,128)(2,1)} %bitcast.73), calls=%async_computation.2 | async-start | bytes 262144 | tf_op jit(solution)/shard_map/all_to_all | solution.py:88
  167.2 7.1 %all-to-all-done.1 = bf16[8,16,512]{2,1,0:T(8,128)(2,1)S(1)} async-done(((bf16[8,16,512]{2,1,0:T(8,128)(2,1)}), bf16[8,16,512]{2,1,0:T(8,128)(2,1)S(1)}, u32[]{:S(2)}, u32[]{:S(2)}) %all-to-all-start.1) | async-done | bytes 131104 | tf_op jit(solution)/shard_map/all_to_all | solution.py:88
  174.3 0.7 gather_fusion
  175.0 0.2 multiply_reduce_fusion.1
  175.3 51.4 %reduce-scatter.5.cloned.1.call-done = bf16[32,512]{1,0:T(8,128)(2,1)} async-done(((bf16[256,512]{1,0:T(8,128)(2,1)}), bf16[32,512]{1,0:T(8,128)(2,1)}) %reduce-scatter.5.cloned.1.call-update) | async-done | bytes 32784 | tf_op jit(solution)/shard_map/reduce_scatter | solution.py:169
  226.7 1.4 add_convert_fusion
  (68 shorter events, 2.2 us)
Async XLA Ops:
  7.2 14.7 %copy-start = (bf16[256,2048]{1,0:T(8,128)(2,1)S(1)}, bf16[256,2048]{1,0:T(8,128)(2,1)}, u32[]{:S(2)}) copy-start(bf16[256,2048]{1,0:T(8,128)(2,1)} %param.27) | copy-start | bytes 3145732
  7.2 50.9 %all-reduce.4.cloned.1.call-start = ((), (), s32[]{:S(2)}) async-start(), calls=%async_computation.4 | async-start | bytes 262144 | tf_op jit(solution)/shard_map/psum | solution.py:148
  12.0 9.9 %copy-start.1 = (bf16[32,2048]{1,0:T(8,128)(2,1)S(1)}, bf16[32,2048]{1,0:T(8,128)(2,1)}, u32[]{:S(2)}) copy-start(bf16[32,2048]{1,0:T(8,128)(2,1)} %param.20) | copy-start | bytes 393220
  12.0 9.9 %copy-start.2 = (bf16[2048,256]{1,0:T(8,128)(2,1)S(1)}, bf16[2048,256]{1,0:T(8,128)(2,1)}, u32[]{:S(2)}) copy-start(bf16[2048,256]{1,0:T(8,128)(2,1)} %param.25) | copy-start | bytes 3145732
  15.4 8.0 %copy-start.11 = (s32[32,2]{0,1:T(2,128)S(1)}, s32[32,2]{0,1:T(2,128)}, u32[]{:S(2)}) copy-start(s32[32,2]{0,1:T(2,128)} %param.35) | copy-start | bytes 772
  15.5 8.5 %copy-start.9 = (bf16[2048]{0:T(1024)(128)(2,1)S(1)}, bf16[2048]{0:T(1024)(128)(2,1)}, u32[]{:S(2)}) copy-start(bf16[2048]{0:T(1024)(128)(2,1)} %param.30) | copy-start | bytes 12292
  15.5 6.0 %copy-start.5 = (f32[32,2,128]{2,1,0:T(2,128)}, f32[32,2,128]{2,1,0:T(2,128)S(1)}, u32[]{:S(2)}) copy-start(f32[32,2,128]{2,1,0:T(2,128)S(1)} %reshape.238) | copy-start | bytes 98308
  16.0 5.9 %copy-start.7 = (f32[32,2,128]{2,1,0:T(2,128)}, f32[32,2,128]{2,1,0:T(2,128)S(1)}, u32[]{:S(2)}) copy-start(f32[32,2,128]{2,1,0:T(2,128)S(1)} %get-tuple-element.17) | copy-start | bytes 98308
  21.3 82.4 %copy-start.3 = (bf16[512,704]{0,1:T(8,128)(2,1)S(1)}, bf16[512,704]{0,1:T(8,128)(2,1)}, u32[]{:S(2)}) copy-start(bf16[512,704]{0,1:T(8,128)(2,1)} %param.33) | copy-start | bytes 2162692
  23.4 81.5 %copy-start.4 = (bf16[512,704]{0,1:T(8,128)(2,1)S(1)}, bf16[512,704]{0,1:T(8,128)(2,1)}, u32[]{:S(2)}) copy-start(bf16[512,704]{0,1:T(8,128)(2,1)} %param.32) | copy-start | bytes 2162692
  61.5 44.6 %all-to-all-start = ((bf16[8,16,2048]{2,1,0:T(8,128)(2,1)}), bf16[8,16,2048]{2,1,0:T(8,128)(2,1)S(1)}, u32[]{:S(2)}, u32[]{:S(2)}) async-start(bf16[8,16,2048]{2,1,0:T(8,128)(2,1)} %bitcast.4), calls=%async_computation | async-start | bytes 1048576 | tf_op jit(solution)/shard_map/all_to_all | solution.py:78
  67.0 70.2 %all-reduce.6.cloned.1.call-start = ((), (), s32[]{:S(2)}) async-start(), calls=%async_computation.7 | async-start | bytes 1441792 | tf_op jit(solution)/shard_map/psum | solution.py:166
  106.0 55.4 %reduce-scatter.3.cloned.1.call-start = ((), (), s32[]{:S(2)}) async-start(), calls=%async_computation.5 | async-start | bytes 655360 | tf_op jit(solution)/shard_map/reduce_scatter | solution.py:85
  109.0 5.9 %copy-start.6 = (f32[32,2,128]{2,1,0:T(2,128)S(1)}, f32[32,2,128]{2,1,0:T(2,128)}, u32[]{:S(2)}) copy-start(f32[32,2,128]{2,1,0:T(2,128)} %copy-done.5) | copy-start | bytes 98308
  109.0 5.9 %copy-start.8 = (f32[32,2,128]{2,1,0:T(2,128)S(1)}, f32[32,2,128]{2,1,0:T(2,128)}, u32[]{:S(2)}) copy-start(f32[32,2,128]{2,1,0:T(2,128)} %copy-done.7) | copy-start | bytes 98308
  114.6 112.0 %reduce-scatter.5.cloned.1.call-start = ((), (), s32[]{:S(2)}) async-start(), calls=%async_computation.6 | async-start | bytes 294912 | tf_op jit(solution)/shard_map/reduce_scatter | solution.py:169
  114.9 22.3 %copy-start.13 = (bf16[704,512]{1,0:T(8,128)(2,1)S(1)}, bf16[704,512]{1,0:T(8,128)(2,1)}, u32[]{:S(2)}) copy-start(bf16[704,512]{1,0:T(8,128)(2,1)} %param.34) | copy-start | bytes 2162692
  119.2 47.7 %copy-start.10 = (bf16[2048]{0:T(1024)(128)(2,1)S(1)}, bf16[2048]{0:T(1024)(128)(2,1)}, u32[]{:S(2)}) copy-start(bf16[2048]{0:T(1024)(128)(2,1)} %param.31) | copy-start | bytes 12292
  119.2 47.7 %copy-start.12 = (bf16[32,2]{0,1:T(2,128)(2,1)S(1)}, bf16[32,2]{0,1:T(2,128)(2,1)}, u32[]{:S(2)}) copy-start(bf16[32,2]{0,1:T(2,128)(2,1)} %param.36) | copy-start | bytes 388
  161.4 12.9 %all-to-all-start.1 = ((bf16[8,16,512]{2,1,0:T(8,128)(2,1)}), bf16[8,16,512]{2,1,0:T(8,128)(2,1)S(1)}, u32[]{:S(2)}, u32[]{:S(2)}) async-start(bf16[8,16,512]{2,1,0:T(8,128)(2,1)} %bitcast.73), calls=%async_computation.2 | async-start | bytes 262144 | tf_op jit(solution)/shard_map/all_to_all | solution.py:88
Sparse Core Ops, SparseCore 0:
  23.5 34.4 all-reduce.3
  106.1 31.0 all-reduce.5
  139.7 21.6 reduce-scatter.2
  164.6 62.0 reduce-scatter.4
where the time goes:
time: 235 us
  waiting for transfers between devices  132 us (56%)
  blocking collectives  36.6 us (16%)
  matrix products  26 us (11%)
  between operations  14.2 us (6%)
  other arithmetic  12.6 us (5%)
  starting transfers between devices  11.2 us (5%)
    reduce_scatter x1, waiting for transfers between devices, per_device(): lax.psum_scatter(jnp.dot(dense_hidden, dense_down, preferred_element_type...  51.4 us
    all_gather x1, blocking collectives, per_device(): lax.all_gather(own_columns(normed_mid), 'ep', axis=0, tiled=True)  36.6 us
    psum x1, waiting for transfers between devices, per_device(): lax.psum(partial_value.astype(jnp.bfloat16), 'tp').astype(jnp.float32)  34.1 us
    reduce_scatter x1, waiting for transfers between devices, padded_experts(): lax.psum_scatter(partial_value.astype(jnp.bfloat16), 'tp', scatter_dimens...  21.9 us
    psum x1, waiting for transfers between devices, per_device(): lax.psum(up_part.astype(jnp.bfloat16), 'tp').astype(jnp.float32)  18 us
    all_to_all x1, waiting for transfers between devices, padded_experts(): lax.all_to_all(summed.reshape(sources, items, summed.shape[1]), 'ep', spl...  7.07 us
    dot_general x1, matrix products, padded_experts(): jnp.dot(hidden_e, expert_down[0], preferred_element_type=jnp.float32)  5.62 us
    all_to_all x1, starting transfers between devices, padded_experts(): lax.all_to_all(summed.reshape(sources, items, summed.shape[1]), 'ep', spl...  5.51 us
  transfers between devices with their start and end apart: 6, of which 5 were waited for; matrix products, arithmetic and copies ran while one was open for 8% of the time, Pallas kernels for 0%

commit v1 on v0

--- a/solution.py
+++ b/solution.py
@@ -145,7 +145,9 @@
         head_gain,
     )
     partial_value = jnp.dot(retained, w_output, preferred_element_type=jnp.float32)
-    attention = lax.psum(partial_value.astype(jnp.bfloat16), "tp").astype(jnp.float32)
+    attention = jnp.sum(lax.all_gather(partial_value.astype(jnp.bfloat16), "tp"), axis=0).astype(
+        jnp.float32
+    )
     middle = resid.astype(jnp.float32) + attention
     normed_mid = rms_norm(middle, ffn_gain).astype(jnp.bfloat16)
     mixing = jax.nn.sigmoid(jnp.dot(normed_mid, w_mix[:, None], preferred_element_type=jnp.float32))

time: 235 us -> 212 us (0.902)
  waiting for transfers between devices: 132 us -> 98.7 us
  blocking collectives: 36.6 us -> 46.8 us
    psum x1 -> x0, waiting for transfers between devices: 34.1 us -> none  [per_device(): lax.psum(partial_value.astype(jnp.bfloat16), 'tp').astype(jnp.float32)]
    all_gather x0 -> x1, blocking collectives: none -> 8.81 us  [per_device(): lax.all_gather(partial_value.astype(jnp.bfloat16), 'tp')]
  transfers between devices with their start and end apart: 6 -> 5, of which waited for: 5 -> 4; matrix products, arithmetic and copies ran while one was open for 8% -> 9% of each run, Pallas kernels for 0% -> 0%
where the time goes in v1:
time: 212 us; the launch traced here: 211 us
  waiting for transfers between devices  98.7 us (47%)
  blocking collectives  46.8 us (22%)
  matrix products  25.9 us (12%)
  between operations  14.1 us (7%)
  other arithmetic  12.2 us (6%)
  starting transfers between devices  11.4 us (5%)
  local copies, waits for them, and re-layouts  2.34 us (1%)
    reduce_scatter x1, waiting for transfers between devices, per_device(): lax.psum_scatter(jnp.dot(dense_hidden, dense_down, preferred_element_type...  51.5 us
    all_gather x1, blocking collectives, per_device(): lax.all_gather(own_columns(normed_mid), 'ep', axis=0, tiled=True)  38 us
    reduce_scatter x1, waiting for transfers between devices, padded_experts(): lax.psum_scatter(partial_value.astype(jnp.bfloat16), 'tp', scatter_dimens...  21.9 us
    psum x1, waiting for transfers between devices, per_device(): lax.psum(up_part.astype(jnp.bfloat16), 'tp').astype(jnp.float32)  18.2 us
    all_gather x1, blocking collectives, per_device(): lax.all_gather(partial_value.astype(jnp.bfloat16), 'tp')  8.81 us
    all_to_all x1, waiting for transfers between devices, padded_experts(): lax.all_to_all(summed.reshape(sources, items, summed.shape[1]), 'ep', spl...  7.08 us
    all_to_all x1, starting transfers between devices, padded_experts(): lax.all_to_all(outgoing, 'ep', split_axis=0, concat_axis=0, tiled=True)  5.81 us
    dot_general x1, matrix products, padded_experts(): jnp.dot(hidden_e, expert_down[0], preferred_element_type=jnp.float32)  5.62 us
  transfers between devices with their start and end apart: 5, of which 4 were waited for; matrix products, arithmetic and copies ran while one was open for 9% of the time, Pallas kernels for 0%

profile of v1, /device:TPU:0, one launch (start us, length us, event | category | flops | bytes accessed | tf_op | source)
XLA Modules:
  0.0 211.5 jit_solution(18385367670551576829)
XLA Ops:
  7.2 0.7 convert_element_type.113
  8.0 1.0 fusion.40
  9.0 0.7 convert_element_type.117
  9.7 0.7 convert_element_type.108
  10.4 0.7 convert_element_type.122
  11.1 0.8 copy.25
  12.1 0.2 select_reduce_fusion
  12.3 0.6 multiply_add_fusion.3
  12.9 1.6 fusion.20
  14.6 1.7 fusion.19
  16.3 1.6 fusion.18
  18.4 5.3 %fusion.61 = f32[32,2,1,128]{3,2,1,0:T(1,128)S(1)} fusion(f32[32,2,128,1]{2,3,1,0:T(1,128)S(1)} %bitcast.74, f32[32,2,128,128]{3,2,1,0:T(8,128)} %param.28), kind=kOutput, calls=%fused_computation.95 | convolution fusion | flops 12582912 | bytes 4259840 | tf_op jit(solution)/shard_map/shd,shde->she/dot_general | solution.py:40
  23.7 0.2 fusion.60
  24.4 0.8 convolution_convert_fusion.1
  25.2 8.8 %all-gather = bf16[128,2048]{1,0:T(8,128)(2,1)S(1)} all-gather(bf16[32,2048]{1,0:T(8,128)(2,1)S(1)} %convolution_convert_fusion.1), channel_id=2, replica_groups=mesh['ep'=8,'tp'=4] {'tp'}, dimensions={0}, use_global_device_ids=true | all-gather | bytes 655360 | tf_op jit(solution)/shard_map/all_gather | solution.py:148
  34.6 1.8 convolution_convert_fusion
  36.3 5.8 %all-to-all-start = ((bf16[8,16,2048]{2,1,0:T(8,128)(2,1)}), bf16[8,16,2048]{2,1,0:T(8,128)(2,1)S(1)}, u32[]{:S(2)}, u32[]{:S(2)}) async-start(bf16[8,16,2048]{2,1,0:T(8,128)(2,1)} %bitcast.5), calls=%async_computation | async-start | bytes 1048576 | tf_op jit(solution)/shard_map/all_to_all | solution.py:78
  42.2 38.0 %all_gather.11 = bf16[256,512]{1,0:T(8,128)(2,1)S(1)} all-gather(bf16[32,512]{1,0:T(8,128)(2,1)S(1)} %constant_dynamic-slice_fusion), channel_id=1, replica_groups=mesh['ep'=8,'tp'=4] {'ep'}, dimensions={0}, use_global_device_ids=true | all-gather | bytes 294912 | tf_op jit(solution)/shard_map/all_gather | solution.py:160
  80.2 1.1 convolution_convert_fusion.2
  81.3 1.1 convolution_convert_fusion.3
  82.5 2.9 %fusion.5 = f32[128,1024]{1,0:T(8,128)S(1)} fusion(bf16[128,2048]{1,0:T(8,128)(2,1)S(1)} %bitcast.70, bf16[1,2048,1024]{2,1,0:T(8,128)(2,1)} %param.37), kind=kOutput, calls=%fused_computation.6 | convolution fusion | flops 536870912 | bytes 5242880 | tf_op jit(solution)/shard_map/dot_general | solution.py:58
  85.5 5.6 %fusion.7 = bf16[128,2048]{1,0:T(8,128)(2,1)} fusion(bf16[1,1024,2048]{2,1,0:T(8,128)(2,1)} %param.39, bf16[128,2048]{1,0:T(8,128)(2,1)S(1)} %bitcast.71, bf16[1,2048,1024]{2,1,0:T(8,128)(2,1)} %param.38, f32[128,1024]{1,0:T(8,128)S(1)} %fusion.5), kind=kOutput, calls=%fused_computation.9 | convolution fusion | flops 1074790400 | bytes 9961472 | tf_op jit(solution)/shard_map/dot_general | solution.py:84
  91.4 4.3 %multiply_add_fusion = f32[32,2,128,128]{3,2,1,0:T(8,128)} fusion(f32[32,2,128,128]{3,2,1,0:T(8,128)} %param.28, f32[32,2,128]{2,1,0:T(2,128)S(1)} %copy-done.6, f32[32,2,128]{2,1,0:T(2,128)S(1)} %copy-done.8, f32[2]{0:T(128)S(1)} %exponential_subtract_fusion), kind=kLoop, calls=%fused_computation.8 | loop fusion | flops 3145728 | bytes 8454152 | tf_op jit(solution)/shard_map/add | solution.py:45
  95.7 18.2 %all-reduce.3.cloned.1.call-done = (bf16[256,704]{0,1:T(8,128)(2,1)}, bf16[256,704]{0,1:T(8,128)(2,1)}) async-done(((bf16[256,704]{0,1:T(8,128)(2,1)}, bf16[256,704]{0,1:T(8,128)(2,1)}), (bf16[256,704]{0,1:T(8,128)(2,1)}, bf16[256,704]{0,1:T(8,128)(2,1)})) %all-reduce.3.cloned.1.call-update) | async-done | bytes 720912 | tf_op jit(solution)/shard_map/psum | solution.py:168
  113.9 2.2 %convolution_convert_fusion.4 = bf16[256,512]{1,0:T(8,128)(2,1)} fusion(bf16[704,512]{1,0:T(8,128)(2,1)S(1)} %copy-done.12, bf16[256,704]{0,1:T(8,128)(2,1)} %get-tuple-element.2, bf16[256,704]{0,1:T(8,128)(2,1)} %get-tuple-element.3), kind=kOutput, calls=%fused_computation.16 | convolution fusion | flops 186122240 | bytes 1703936 | tf_op jit(solution)/shard_map/dot_general | solution.py:172
  116.2 21.9 %reduce-scatter.3.cloned.1.call-done = bf16[128,512]{1,0:T(8,128)(2,1)} async-done(((bf16[128,2048]{1,0:T(8,128)(2,1)}), bf16[128,512]{1,0:T(8,128)(2,1)}) %reduce-scatter.3.cloned.1.call-update) | async-done | bytes 131088 | tf_op jit(solution)/shard_map/reduce_scatter | solution.py:85
  138.1 5.5 %all-to-all-start.1 = ((bf16[8,16,512]{2,1,0:T(8,128)(2,1)}), bf16[8,16,512]{2,1,0:T(8,128)(2,1)S(1)}, u32[]{:S(2)}, u32[]{:S(2)}) async-start(bf16[8,16,512]{2,1,0:T(8,128)(2,1)} %bitcast.75), calls=%async_computation.2 | async-start | bytes 262144 | tf_op jit(solution)/shard_map/all_to_all | solution.py:88
  143.9 7.1 %all-to-all-done.1 = bf16[8,16,512]{2,1,0:T(8,128)(2,1)S(1)} async-done(((bf16[8,16,512]{2,1,0:T(8,128)(2,1)}), bf16[8,16,512]{2,1,0:T(8,128)(2,1)S(1)}, u32[]{:S(2)}, u32[]{:S(2)}) %all-to-all-start.1) | async-done | bytes 131104 | tf_op jit(solution)/shard_map/all_to_all | solution.py:88
  151.0 0.7 gather_fusion
  151.7 0.2 multiply_reduce_fusion.1
  152.0 51.5 %reduce-scatter.5.cloned.1.call-done = bf16[32,512]{1,0:T(8,128)(2,1)} async-done(((bf16[256,512]{1,0:T(8,128)(2,1)}), bf16[32,512]{1,0:T(8,128)(2,1)}) %reduce-scatter.5.cloned.1.call-update) | async-done | bytes 32784 | tf_op jit(solution)/shard_map/reduce_scatter | solution.py:171
  203.5 1.4 add_convert_fusion
  (65 shorter events, 2.5 us)
Async XLA Ops:
  7.2 17.2 %copy-start = (bf16[256,2048]{1,0:T(8,128)(2,1)S(1)}, bf16[256,2048]{1,0:T(8,128)(2,1)}, u32[]{:S(2)}) copy-start(bf16[256,2048]{1,0:T(8,128)(2,1)} %param.27) | copy-start | bytes 3145732
  14.5 9.8 %copy-start.1 = (bf16[32,2048]{1,0:T(8,128)(2,1)S(1)}, bf16[32,2048]{1,0:T(8,128)(2,1)}, u32[]{:S(2)}) copy-start(bf16[32,2048]{1,0:T(8,128)(2,1)} %param.20) | copy-start | bytes 393220
  14.5 9.8 %copy-start.2 = (bf16[2048,256]{1,0:T(8,128)(2,1)S(1)}, bf16[2048,256]{1,0:T(8,128)(2,1)}, u32[]{:S(2)}) copy-start(bf16[2048,256]{1,0:T(8,128)(2,1)} %param.25) | copy-start | bytes 3145732
  18.0 6.2 %copy-start.5 = (f32[32,2,128]{2,1,0:T(2,128)}, f32[32,2,128]{2,1,0:T(2,128)S(1)}, u32[]{:S(2)}) copy-start(f32[32,2,128]{2,1,0:T(2,128)S(1)} %reshape.238) | copy-start | bytes 98308
  18.4 5.9 %copy-start.7 = (f32[32,2,128]{2,1,0:T(2,128)}, f32[32,2,128]{2,1,0:T(2,128)S(1)}, u32[]{:S(2)}) copy-start(f32[32,2,128]{2,1,0:T(2,128)S(1)} %get-tuple-element.17) | copy-start | bytes 98308
  23.7 56.5 %copy-start.3 = (bf16[512,704]{0,1:T(8,128)(2,1)S(1)}, bf16[512,704]{0,1:T(8,128)(2,1)}, u32[]{:S(2)}) copy-start(bf16[512,704]{0,1:T(8,128)(2,1)} %param.33) | copy-start | bytes 2162692
  25.1 56.2 %copy-start.4 = (bf16[512,704]{0,1:T(8,128)(2,1)S(1)}, bf16[512,704]{0,1:T(8,128)(2,1)}, u32[]{:S(2)}) copy-start(bf16[512,704]{0,1:T(8,128)(2,1)} %param.32) | copy-start | bytes 2162692
  36.3 46.2 %all-to-all-start = ((bf16[8,16,2048]{2,1,0:T(8,128)(2,1)}), bf16[8,16,2048]{2,1,0:T(8,128)(2,1)S(1)}, u32[]{:S(2)}, u32[]{:S(2)}) async-start(bf16[8,16,2048]{2,1,0:T(8,128)(2,1)} %bitcast.5), calls=%async_computation | async-start | bytes 1048576 | tf_op jit(solution)/shard_map/all_to_all | solution.py:78
  42.1 71.8 %all-reduce.3.cloned.1.call-start = ((), (), s32[]{:S(2)}) async-start(), calls=%async_computation.6 | async-start | bytes 1441792 | tf_op jit(solution)/shard_map/psum | solution.py:168
  82.5 55.6 %reduce-scatter.3.cloned.1.call-start = ((), (), s32[]{:S(2)}) async-start(), calls=%async_computation.4 | async-start | bytes 655360 | tf_op jit(solution)/shard_map/reduce_scatter | solution.py:85
  85.4 5.7 %copy-start.10 = (s32[32,2]{0,1:T(2,128)S(1)}, s32[32,2]{0,1:T(2,128)}, u32[]{:S(2)}) copy-start(s32[32,2]{0,1:T(2,128)} %param.35) | copy-start | bytes 772
  85.5 5.9 %copy-start.6 = (f32[32,2,128]{2,1,0:T(2,128)S(1)}, f32[32,2,128]{2,1,0:T(2,128)}, u32[]{:S(2)}) copy-start(f32[32,2,128]{2,1,0:T(2,128)} %copy-done.5) | copy-start | bytes 98308
  85.5 5.9 %copy-start.8 = (f32[32,2,128]{2,1,0:T(2,128)S(1)}, f32[32,2,128]{2,1,0:T(2,128)}, u32[]{:S(2)}) copy-start(f32[32,2,128]{2,1,0:T(2,128)} %copy-done.7) | copy-start | bytes 98308
  91.1 112.4 %reduce-scatter.5.cloned.1.call-start = ((), (), s32[]{:S(2)}) async-start(), calls=%async_computation.5 | async-start | bytes 294912 | tf_op jit(solution)/shard_map/reduce_scatter | solution.py:171
  91.4 22.5 %copy-start.12 = (bf16[704,512]{1,0:T(8,128)(2,1)S(1)}, bf16[704,512]{1,0:T(8,128)(2,1)}, u32[]{:S(2)}) copy-start(bf16[704,512]{1,0:T(8,128)(2,1)} %param.34) | copy-start | bytes 2162692
  95.7 47.9 %copy-start.9 = (bf16[2048]{0:T(1024)(128)(2,1)S(1)}, bf16[2048]{0:T(1024)(128)(2,1)}, u32[]{:S(2)}) copy-start(bf16[2048]{0:T(1024)(128)(2,1)} %param.31) | copy-start | bytes 12292
  95.7 47.9 %copy-start.11 = (bf16[32,2]{0,1:T(2,128)(2,1)S(1)}, bf16[32,2]{0,1:T(2,128)(2,1)}, u32[]{:S(2)}) copy-start(bf16[32,2]{0,1:T(2,128)(2,1)} %param.36) | copy-start | bytes 388
  138.1 12.9 %all-to-all-start.1 = ((bf16[8,16,512]{2,1,0:T(8,128)(2,1)}), bf16[8,16,512]{2,1,0:T(8,128)(2,1)S(1)}, u32[]{:S(2)}, u32[]{:S(2)}) async-start(bf16[8,16,512]{2,1,0:T(8,128)(2,1)} %bitcast.75), calls=%async_computation.2 | async-start | bytes 262144 | tf_op jit(solution)/shard_map/all_to_all | solution.py:88
Sparse Core Ops, SparseCore 0:
  82.6 31.2 all-reduce.2
  116.4 21.6 reduce-scatter.2
  141.4 62.0 reduce-scatter.4
